TPU v7x, 32 devices: a whole 2x2x4 slice. The times are simulated.
32 devices in a mesh: sp: 4 (over z), fs: 4 (over y, x), tp: 2 (over core).
Axes of the slice: x: 2, y: 2, z: 4, core: 2. Of those that a mesh axis runs over, the one named last changes fastest.
Arguments:
- queries: bfloat16 [4, 1024, 512], P('fs', 'sp', 'tp'), may hold values from -60 to 60
- keys: bfloat16 [4, 1024, 256], P('fs', 'sp', 'tp'), may hold values from -4.5 to 4.5
- values: bfloat16 [4, 1024, 256], P('fs', 'sp', 'tp'), may hold values from -6 to 6
- forget_cache: float32 [4, 1024, 8], P('fs', 'sp', 'tp'), may hold values from -128 to 0, as said below
- fox_gain: float32 [512], P('tp'), may hold values from 0.1 to 1.9
- receptance: bfloat16 [4, 1024, 512], P('fs', 'sp', 'tp'), may hold values from -6 to 6
- lin_keys: bfloat16 [4, 1024, 512], P('fs', 'sp', 'tp'), may hold values from -6 to 6
- lin_values: bfloat16 [4, 1024, 512], P('fs', 'sp', 'tp'), may hold values from -6 to 6
- learn_logit: bfloat16 [4, 1024, 512], P('fs', 'sp', 'tp'), may hold values from -12 to 4
- decay_log: float32 [4, 1024, 512], P('fs', 'sp', 'tp'), may hold values from -16 to 0
- lin_gain: float32 [512], P('tp'), may hold values from 0.1 to 1.9
- out_fox_weight: bfloat16 [512, 2048], P('tp', 'fs'), may hold values from -0.1875 to 0.1875
- out_lin_weight: bfloat16 [512, 2048], P('tp', 'fs'), may hold values from -0.1875 to 0.1875
Outputs:
- mixed: bfloat16 [4, 1024, 2048], P('fs', ('sp', 'tp'))
Inputs may be any that keep to these rules, and one draw needn't show every extreme that they name: `forget_cache`: Non-increasing along the positions of each sequence and head.
All inputs are finite; a program needn't handle non-finite values.
Results may differ from a plain program's by a relative error of at most 0.017.
Values may be sent and summed in bfloat16 or wider, within the bound.
A program may use at most 64 MiB of HBM per device.

v0:
```python
import math
import jax
import jax.numpy as jnp
from jax import lax
from jax.sharding import PartitionSpec as P

HEAD = 64
SPAN = 64
HIGHEST = lax.Precision.HIGHEST
NORM_EPS = 1e-06


def carried_in(shard, axis, join, neutral):
    place = lax.axis_index(axis)
    gathered = jax.tree.map(
        lambda a, kind: lax.all_gather(a.astype(kind), axis), shard, (jnp.bfloat16, jnp.bfloat16)
    )
    state = jax.tree.map(lambda a, e: jnp.zeros_like(a) + jnp.asarray(e, a.dtype), shard, neutral)

    def one(lap, state):
        return join(
            state,
            jax.tree.map(
                lambda a, own: lax.dynamic_index_in_dim(a, lap, 0, False).astype(own.dtype),
                gathered,
                shard,
            ),
        )

    return lax.fori_loop(0, place, one, state)


def round_half(tensor):
    return lax.optimization_barrier(tensor.astype(jnp.bfloat16)).astype(jnp.float32)


def forget_attention(query_rows, key_rows, value_rows, forget_rows, fox_gain):
    row_count = query_rows.shape[0]
    head_count = query_rows.shape[1] // HEAD
    kv_count = key_rows.shape[1] // HEAD
    group_size = head_count // kv_count
    score_scale = HEAD ** (-0.5)
    own_first = lax.axis_index("sp") * row_count
    forget_all = lax.all_gather(forget_rows, "sp", axis=0, tiled=True)
    forget_own = forget_rows.reshape(row_count, kv_count, group_size)
    query_heads = query_rows.reshape(row_count, kv_count, group_size, HEAD)
    query_pos = own_first + jnp.arange(row_count, dtype=jnp.int32)
    start_state = (
        jnp.full((row_count, kv_count, group_size), -1e30, jnp.float32),
        jnp.zeros((row_count, kv_count, group_size), jnp.float32),
        jnp.zeros((row_count, kv_count, group_size, HEAD), jnp.float32),
    )
    key_piece = lax.all_gather(key_rows, "sp", axis=0, tiled=True)
    value_piece = lax.all_gather(value_rows, "sp", axis=0, tiled=True)
    piece_rows = key_piece.shape[0]
    block_rows = math.gcd(piece_rows, 512)

    def attend(state):

        def one_block(block_index, inner):
            running_max, totals, weighted = inner
            local_first = (block_index * block_rows).astype(jnp.int32)
            key_block = lax.dynamic_slice_in_dim(key_piece, local_first, block_rows, 0).reshape(
                block_rows, kv_count, HEAD
            )
            value_block = lax.dynamic_slice_in_dim(value_piece, local_first, block_rows, 0).reshape(
                block_rows, kv_count, HEAD
            )
            forget_block = lax.dynamic_slice_in_dim(forget_all, local_first, block_rows, 0).reshape(
                block_rows, kv_count, group_size
            )
            key_pos = local_first + jnp.arange(block_rows, dtype=jnp.int32)
            allowed = (key_pos[None, :] <= query_pos[:, None])[:, None, None, :]
            scores = jnp.einsum(
                "tkgd,skd->tkgs", query_heads, key_block, preferred_element_type=jnp.float32
            )
            scores = (
                scores * score_scale
                + forget_own[..., None]
                - jnp.transpose(forget_block, (1, 2, 0))[None]
            )
            scores = jnp.where(allowed, scores, -1e30)
            new_max = jnp.maximum(running_max, jnp.max(scores, axis=-1))
            rescale = jnp.exp(running_max - new_max)
            weights = jnp.where(allowed, jnp.exp(scores - new_max[..., None]), 0.0)
            totals = totals * rescale + jnp.sum(weights, axis=-1)
            update = jnp.einsum(
                "tkgs,skd->tkgd",
                weights.astype(jnp.bfloat16),
                value_block,
                preferred_element_type=jnp.float32,
            )
            weighted = weighted * rescale[..., None] + update
            return (new_max, totals, weighted)

        return lax.fori_loop(0, piece_rows // block_rows, one_block, state)

    def keep_state(running_state):
        return running_state

    running_max, totals, weighted = lax.cond(
        jnp.int32(0) < own_first + row_count, attend, keep_state, start_state
    )
    attended = (weighted / totals[..., None]).reshape(row_count, head_count, HEAD)
    normed = attended * lax.rsqrt(jnp.mean(attended * attended, axis=-1, keepdims=True) + NORM_EPS)
    return (
        (normed * fox_gain.reshape(head_count, HEAD))
        .reshape(row_count, head_count * HEAD)
        .astype(jnp.bfloat16)
    )


def product(left, right, form):
    return jnp.einsum(form, left, right, precision=HIGHEST)


def delta_attention(recept_rows, key_rows, value_rows, learn_rows, decay_rows, lin_gain):
    row_count = recept_rows.shape[0]
    head_count = recept_rows.shape[1] // HEAD
    span_count = row_count // SPAN

    def arrange(tensor):
        return jnp.transpose(
            tensor.astype(jnp.float32).reshape(span_count, SPAN, head_count, HEAD), (0, 2, 1, 3)
        )

    recept = arrange(recept_rows)
    key_float = arrange(key_rows)
    value_float = arrange(value_rows)
    learn_rate = jax.nn.sigmoid(arrange(learn_rows))
    unit_keys = key_float * lax.rsqrt(
        jnp.sum(key_float * key_float, axis=-1, keepdims=True) + NORM_EPS
    )
    log_decay = -jnp.exp(arrange(decay_rows))
    strict_lower = jnp.tril(jnp.ones((SPAN, SPAN), jnp.float32), -1)
    with_diagonal = jnp.tril(jnp.ones((SPAN, SPAN), jnp.float32))
    identity_head = jnp.broadcast_to(jnp.eye(HEAD, dtype=jnp.float32), (head_count, HEAD, HEAD))
    identity_span = jnp.broadcast_to(jnp.eye(SPAN, dtype=jnp.float32), (head_count, SPAN, SPAN))
    zero_state = jnp.zeros((head_count, HEAD, HEAD), jnp.float32)

    def one_span(state, inputs):
        recept_t, key_t, value_t, unit_t, rate_t, fall_t = inputs
        inclusive = jnp.cumsum(fall_t, axis=1)
        grown = jnp.exp(inclusive)
        shrunk = jnp.exp(-inclusive)
        erase_in = -unit_t * jnp.exp(inclusive - fall_t)
        read_in = recept_t * grown
        erase_out = unit_t * rate_t * shrunk
        write_out = key_t * shrunk
        padded_values = jnp.concatenate([value_t, jnp.zeros_like(value_t)], axis=-1)
        mix_erase = product(erase_in, erase_out, "hid,hjd->hij") * strict_lower
        mix_write = product(erase_in, write_out, "hid,hjd->hij") * strict_lower
        read_erase = product(read_in, erase_out, "hid,hjd->hij") * with_diagonal
        read_write = product(read_in, write_out, "hid,hjd->hij") * with_diagonal
        right_side = product(erase_in, state, "hid,hrd->hir") + product(
            mix_write, padded_values, "hij,hjr->hir"
        )
        erased = jax.scipy.linalg.solve_triangular(
            identity_span - mix_erase, right_side, lower=True, unit_diagonal=True
        )
        outputs = (
            product(read_in, state, "hid,hrd->hir")
            + product(read_erase, erased, "hij,hjr->hir")
            + product(read_write, padded_values, "hij,hjr->hir")
        )
        final_grow = grown[:, -1, :]
        state = (
            state * final_grow[:, None, :]
            + product(erased, erase_out * final_grow[:, None, :], "hlr,hld->hrd")
            + product(padded_values, write_out * final_grow[:, None, :], "hlr,hld->hrd")
        )
        return (state, outputs)

    start_state = jnp.concatenate([zero_state, identity_head], axis=1)
    final_state, outputs = lax.scan(
        one_span, start_state, (recept, key_float, value_float, unit_keys, learn_rate, log_decay)
    )
    local_read = outputs[..., :HEAD]
    carried_read = outputs[..., HEAD:]

    def chain(earlier, later):
        return (
            product(earlier[0], later[0], "hij,hjk->hik"),
            product(earlier[1], later[0], "hij,hjk->hik") + later[1],
        )

    entry_map, entry_state = carried_in(
        (final_state[:, HEAD:], final_state[:, :HEAD]), "sp", chain, (identity_head, zero_state)
    )
    readout = local_read + jnp.einsum(
        "hvk,nhtk->nhtv", entry_state, carried_read, precision=HIGHEST
    )
    readout = jnp.transpose(readout, (0, 2, 1, 3)).reshape(row_count, head_count, HEAD)
    centred = readout - jnp.mean(readout, axis=-1, keepdims=True)
    normed = centred * lax.rsqrt(jnp.mean(centred * centred, axis=-1, keepdims=True) + HEAD * 1e-05)
    return (
        (normed * lin_gain.reshape(head_count, HEAD))
        .reshape(row_count, head_count * HEAD)
        .astype(jnp.bfloat16)
    )


def shards(
    queries,
    keys,
    values,
    forget_cache,
    fox_gain,
    receptance,
    lin_keys,
    lin_values,
    learn_logit,
    decay_log,
    lin_gain,
    out_fox_weight,
    out_lin_weight,
):
    fox_out = forget_attention(queries[0], keys[0], values[0], forget_cache[0], fox_gain)
    lin_out = delta_attention(
        receptance[0], lin_keys[0], lin_values[0], learn_logit[0], decay_log[0], lin_gain
    )
    fox_weight, lin_weight = (
        lax.all_gather(out_fox_weight, "fs", axis=1, tiled=True),
        lax.all_gather(out_lin_weight, "fs", axis=1, tiled=True),
    )
    partial_value = jnp.dot(fox_out, fox_weight, preferred_element_type=jnp.float32)
    partial_value = partial_value + jnp.dot(lin_out, lin_weight, preferred_element_type=jnp.float32)
    summed = lax.psum_scatter(
        round_half(partial_value).astype(jnp.bfloat16), "tp", scatter_dimension=0, tiled=True
    )
    return summed[None]


def solution(mesh):
    return jax.shard_map(
        shards,
        mesh=mesh,
        in_specs=(
            P("fs", "sp", "tp"),
            P("fs", "sp", "tp"),
            P("fs", "sp", "tp"),
            P("fs", "sp", "tp"),
            P("tp"),
            P("fs", "sp", "tp"),
            P("fs", "sp", "tp"),
            P("fs", "sp", "tp"),
            P("fs", "sp", "tp"),
            P("fs", "sp", "tp"),
            P("tp"),
            P("tp", "fs"),
            P("tp", "fs"),
        ),
        out_specs=P("fs", ("sp", "tp"), None),
        check_vma=False,
    )
```

profile of v0, /device:TPU:0, one launch (start us, length us, event | category | flops | bytes accessed | tf_op | source)
XLA Modules:
  0.0 230.0 jit_solution(1138776864522754009)
XLA Ops:
  6.5 0.7 all-gather.8.cloned.1.call-update
  7.3 0.7 all-gather.10.cloned.1.call-update
  8.1 1.2 reshape.164
  10.2 1.1 reshape.163
  11.3 1.0 neg.24
  13.0 106.6 %while.46 = (s32[]{:T(128)}, f32[4,128,64]{1,2,0:T(8,128)S(1)}, f32[4,4,64,128]{3,2,1,0:T(8,128)}, f32[4,4,64,64]{3,1,2,0:T(4,128)}, f32[4,4,64,64]{3,1,2,0:T(4,...) while((s32[]{:T(128)}, f32[4,128,64]{1,2,0:T(8,128)S(1)}, ...), condition=%wide.region_10.11_spmd.clone.clone, body=%wide.region_8.10_spmd.clone.clone.sunk | while | flops 253308992 | bytes 5993869 | solution.py:175
  13.0 0.9 constant_dynamic-slice_fusion.20
  14.1 0.9 constant_dynamic-slice_fusion.19
  15.6 19.7 %custom-call.11 = f32[4,1,64,64]{2,3,1,0:T(8,128)S(1)} custom-call(f32[4,1,64,64]{3,2,1,0:T(8,128)S(1)} %fusion.172), custom_call_target="InvertDiagBlocksLowerTriangular" | custom-call | tf_op jit(solution)/shard_map/while/body/eval_jaxpr/jit(_solve_triangular)/vmap()/triangular_solve | solution.py:158
  37.9 0.9 fusion.176
  39.2 0.4 convolution_add_fusion.12
  39.6 0.9 constant_dynamic-slice_fusion.20
  40.7 0.9 constant_dynamic-slice_fusion.19
  42.2 19.7 %custom-call.11 = f32[4,1,64,64]{2,3,1,0:T(8,128)S(1)} custom-call(f32[4,1,64,64]{3,2,1,0:T(8,128)S(1)} %fusion.172), custom_call_target="InvertDiagBlocksLowerTriangular" | custom-call | tf_op jit(solution)/shard_map/while/body/eval_jaxpr/jit(_solve_triangular)/vmap()/triangular_solve | solution.py:158
  64.5 0.9 fusion.176
  65.9 0.4 convolution_add_fusion.12
  66.3 0.9 constant_dynamic-slice_fusion.20
  67.4 0.9 constant_dynamic-slice_fusion.19
  68.9 19.7 %custom-call.11 = f32[4,1,64,64]{2,3,1,0:T(8,128)S(1)} custom-call(f32[4,1,64,64]{3,2,1,0:T(8,128)S(1)} %fusion.172), custom_call_target="InvertDiagBlocksLowerTriangular" | custom-call | tf_op jit(solution)/shard_map/while/body/eval_jaxpr/jit(_solve_triangular)/vmap()/triangular_solve | solution.py:158
  91.2 0.9 fusion.176
  92.5 0.4 convolution_add_fusion.12
  92.9 0.9 constant_dynamic-slice_fusion.20
  94.0 0.9 constant_dynamic-slice_fusion.19
  95.5 19.7 %custom-call.11 = f32[4,1,64,64]{2,3,1,0:T(8,128)S(1)} custom-call(f32[4,1,64,64]{3,2,1,0:T(8,128)S(1)} %fusion.172), custom_call_target="InvertDiagBlocksLowerTriangular" | custom-call | tf_op jit(solution)/shard_map/while/body/eval_jaxpr/jit(_solve_triangular)/vmap()/triangular_solve | solution.py:158
  117.8 0.9 fusion.176
  119.2 0.4 convolution_add_fusion.12
  119.7 15.7 %all-gather.3 = bf16[16,64,64]{2,1,0:T(8,128)(2,1)S(1)} all-gather(bf16[4,64,64]{2,1,0:T(8,128)(2,1)S(1)} %get-tuple-element.533), channel_id=5, replica_groups=mesh['sp'=4,'fs'=4,'tp'=2] {'sp'}, dimensions={0}, use_global_device_ids=true | all-gather | bytes 163840 | tf_op jit(solution)/shard_map/all_gather | solution.py:16
  135.4 14.6 %all-gather.4 = bf16[16,64,64]{2,1,0:T(8,128)(2,1)S(1)} all-gather(bf16[4,64,64]{2,1,0:T(8,128)(2,1)S(1)} %get-tuple-element.532), channel_id=6, replica_groups=mesh['sp'=4,'fs'=4,'tp'=2] {'sp'}, dimensions={0}, use_global_device_ids=true | all-gather | bytes 163840 | tf_op jit(solution)/shard_map/all_gather | solution.py:16
  150.0 1.0 copy-done
  151.4 1.7 fusion.65
  153.7 0.8 copy.73
  154.9 0.8 copy.72
  156.0 13.2 %all-gather.1 = f32[1,1024,4]{1,2,0:T(4,128)S(1)} all-gather(f32[1,256,4]{1,2,0:T(4,128)S(1)} %copy-done.10), channel_id=3, replica_groups=mesh['sp'=4,'fs'=4,'tp'=2] {'sp'}, dimensions={1}, use_global_device_ids=true | all-gather | bytes 20480 | tf_op jit(solution)/shard_map/all_gather | solution.py:44
  169.2 14.5 %all-gather = bf16[1,1024,128]{1,2,0:T(8,128)(2,1)S(1)} all-gather(bf16[1,256,128]{1,2,0:T(8,128)(2,1)S(1)} %copy.55), channel_id=2, replica_groups=mesh['sp'=4,'fs'=4,'tp'=2] {'sp'}, dimensions={1}, use_global_device_ids=true | all-gather | bytes 327680 | tf_op jit(solution)/shard_map/all_gather | solution.py:53
  183.7 14.0 %all-gather.2 = bf16[1,1024,128]{1,2,0:T(8,128)(2,1)S(1)} all-gather(bf16[1,256,128]{1,2,0:T(8,128)(2,1)S(1)} %copy.56), channel_id=4, replica_groups=mesh['sp'=4,'fs'=4,'tp'=2] {'sp'}, dimensions={1}, use_global_device_ids=true | all-gather | bytes 327680 | tf_op jit(solution)/shard_map/all_gather | solution.py:54
  197.7 10.5 %conditional.1 = (f32[256,2,2]{0,2,1:T(2,128)}, f32[256,2,2,64]{0,3,2,1:T(8,128)}) conditional(s32[]{:T(128)} %convert_element_type.58, () %tuple.38, (s32[]{:T(128)}, s32[256]{0:T(256)S(1)}, bf16[1,256,256]{2,1,0:T(8,128)(2,1)S(1)}, bf16[1024,128]{0,1:T(8,128)(2,1)S(1)}, f32[1,256,4]{1,2,0:T(4,128)S(1)}, /*index=5*/f32[1024,4]{0,1:T(4,128)S(1)}, ...), branch_computations={%region_0.0_spmd, %region_1.6_spmd} | conditional | flops 140318464 | bytes 8662403 | solution.py:101
  197.7 0.8 copy.57
  198.5 9.7 %while.44 = (s32[]{:T(128)}, f32[256,2,2]{0,2,1:T(2,128)S(1)}, f32[256,2,2]{0,2,1:T(2,128)}, f32[256,2,2,64]{0,3,2,1:T(8,128)}, s32[256]{0:T(256)S(1)}, /*index=...) while((s32[]{:T(128)}, f32[256,2,2]{0,2,1:T(2,128)S(1)}, ...), condition=%wide.wide.region_5.5_spmd.clone, body=%wide.wide.region_2.4_spmd.clone.sunk | while | flops 140318208 | bytes 8373459 | solution.py:96
  198.7 1.6 fusion.181
  200.7 0.6 fusion.184
  201.4 1.2 fusion.185
  202.8 1.6 fusion.181
  204.8 1.3 fusion.184
  206.1 2.1 fusion.185
  208.2 1.1 multiply_reduce_fusion.2
  209.5 1.7 fusion.67
  211.2 2.7 %fusion.54 = bf16[256,2048]{1,0:T(8,128)(2,1)} fusion(f32[256,2048]{1,0:T(8,128)S(1)} %fusion.67, bf16[256,2048]{1,0:T(8,128)(2,1)} %all-gather.10.cloned.1.call-done, f32[256,256]{1,0:T(8,128)S(1)} %copy-done.1, f32[256,256]{1,0:T(8,128)S(1)} %reshape.160, f32[256,256]{1,0:T(8,128)S(1)} %copy-done.2, f32[256]{0:T(256)S(1)} %copy-done.13), kind=kOutput, calls=%fused_computation.87 | convolution fusion | flops 269746176 | bytes 4981760 | tf_op jit(solution)/shard_map/dot_general | solution.py:227
  213.9 9.5 %reduce-scatter.2.cloned.1.call-done = bf16[128,2048]{1,0:T(8,128)(2,1)} async-done(((bf16[256,2048]{1,0:T(8,128)(2,1)}), bf16[128,2048]{1,0:T(8,128)(2,1)}) %reduce-scatter.2.cloned.1.call-update) | async-done | bytes 524304 | tf_op jit(solution)/shard_map/reduce_scatter | solution.py:228
  (167 shorter events, 19.3 us)
Async XLA Ops:
  6.5 3.6 %copy-start.4 = (bf16[1,256,256]{2,1,0:T(8,128)(2,1)S(1)}, bf16[1,256,256]{2,1,0:T(8,128)(2,1)}, u32[]{:S(2)}) copy-start(bf16[1,256,256]{2,1,0:T(8,128)(2,1)} %param.29) | copy-start | bytes 393220
  6.5 202.9 %all-gather.8.cloned.1.call-start = ((), (), s32[]{:S(2)}) async-start(), calls=%async_computation.1 | async-start | bytes 1310720 | tf_op jit(solution)/shard_map/all_gather | solution.py:223
  7.3 4.0 %copy-start.3 = (f32[1,256,256]{2,1,0:T(8,128)S(1)}, f32[1,256,256]{2,1,0:T(8,128)}, u32[]{:S(2)}) copy-start(f32[1,256,256]{2,1,0:T(8,128)} %param.30) | copy-start | bytes 786436
  7.3 203.9 %all-gather.10.cloned.1.call-start = ((), (), s32[]{:S(2)}) async-start(), calls=%async_computation.2 | async-start | bytes 1310720 | tf_op jit(solution)/shard_map/all_gather | solution.py:224
  8.0 215.4 %reduce-scatter.2.cloned.1.call-start = ((), (), s32[]{:S(2)}) async-start(), calls=%async_computation.3 | async-start | bytes 1572864 | tf_op jit(solution)/shard_map/reduce_scatter | solution.py:228
  9.6 2.7 %copy-start.5 = (bf16[1,256,256]{2,1,0:T(8,128)(2,1)S(1)}, bf16[1,256,256]{2,1,0:T(8,128)(2,1)}, u32[]{:S(2)}) copy-start(bf16[1,256,256]{2,1,0:T(8,128)(2,1)} %param.28) | copy-start | bytes 393220
  9.7 2.9 %copy-start.6 = (bf16[1,256,256]{2,1,0:T(8,128)(2,1)S(1)}, bf16[1,256,256]{2,1,0:T(8,128)(2,1)}, u32[]{:S(2)}) copy-start(bf16[1,256,256]{2,1,0:T(8,128)(2,1)} %param.26) | copy-start | bytes 393220
  150.0 1.0 copy-start
  153.1 2.7 %copy-start.8 = (bf16[1,256,128]{2,1,0:T(8,128)(2,1)S(1)}, bf16[1,256,128]{2,1,0:T(8,128)(2,1)}, u32[]{:S(2)}) copy-start(bf16[1,256,128]{2,1,0:T(8,128)(2,1)} %param.22) | copy-start | bytes 196612
  153.1 2.8 %copy-start.9 = (bf16[1,256,128]{2,1,0:T(8,128)(2,1)S(1)}, bf16[1,256,128]{2,1,0:T(8,128)(2,1)}, u32[]{:S(2)}) copy-start(bf16[1,256,128]{2,1,0:T(8,128)(2,1)} %param.23) | copy-start | bytes 196612
  153.1 2.9 %copy-start.10 = (f32[1,256,4]{1,2,0:T(4,128)S(1)}, f32[1,256,4]{1,2,0:T(4,128)}, u32[]{:S(2)}) copy-start(f32[1,256,4]{1,2,0:T(4,128)} %param.24) | copy-start | bytes 12292
  153.4 44.3 %copy-start.7 = (bf16[1,256,256]{2,1,0:T(8,128)(2,1)S(1)}, bf16[1,256,256]{2,1,0:T(8,128)(2,1)}, u32[]{:S(2)}) copy-start(bf16[1,256,256]{2,1,0:T(8,128)(2,1)} %param.21) | copy-start | bytes 393220
  197.7 11.6 %copy-start.12 = (f32[256]{0:T(256)S(1)}, f32[256]{0:T(256)}, u32[]{:S(2)}) copy-start(f32[256]{0:T(256)} %param.25) | copy-start | bytes 3076
  197.7 0.8 copy-start.11
  208.2 3.0 %copy-start.1 = (f32[256,256]{1,0:T(8,128)S(1)}, f32[256,256]{1,0:T(8,128)}, u32[]{:S(2)}) copy-start(f32[256,256]{1,0:T(8,128)} %copy.73) | copy-start | bytes 786436
  208.2 3.0 %copy-start.2 = (f32[256,256]{1,0:T(8,128)S(1)}, f32[256,256]{1,0:T(8,128)}, u32[]{:S(2)}) copy-start(f32[256,256]{1,0:T(8,128)} %copy.72) | copy-start | bytes 786436
  208.2 3.0 %copy-start.13 = (f32[256]{0:T(256)S(1)}, f32[256]{0:T(256)}, u32[]{:S(2)}) copy-start(f32[256]{0:T(256)} %param.31) | copy-start | bytes 3076
Sparse Core Ops, SparseCore 0:
  9.2 29.8 all-gather.7
  40.9 27.0 all-gather.9
  214.0 9.3 reduce-scatter.1
where the time goes:
time: 231 us; the launch traced here: 230 us
  other arithmetic  85.3 us (37%)
  blocking collectives  71.9 us (31%)
  matrix products  30.9 us (13%)
  local copies, waits for them, and re-layouts  16.6 us (7%)
  between operations  13.5 us (6%)
  waiting for transfers between devices  11 us (5%)
    another operation x12, other arithmetic, one_span(): jax.scipy.linalg.solve_triangular(identity_span - mix_erase, right_side,...  79 us
    all_gather x2, blocking collectives, carried_in(): lax.all_gather(a.astype(kind), axis)  30.2 us
    dot_general x44, matrix products, product(): return jnp.einsum(form, left, right, precision=HIGHEST)  16.7 us
    all_gather x1, blocking collectives, forget_attention(): key_piece = lax.all_gather(key_rows, 'sp', axis=0, tiled=True)  14.5 us
    all_gather x1, blocking collectives, forget_attention(): value_piece = lax.all_gather(value_rows, 'sp', axis=0, tiled=True)  14 us
    all_gather x1, blocking collectives, forget_attention(): forget_all = lax.all_gather(forget_rows, 'sp', axis=0, tiled=True)  13.2 us
    reduce_scatter x1, waiting for transfers between devices, shards(): lax.psum_scatter(round_half(partial_value).astype(jnp.bfloat16), 'tp', sc...  9.53 us
    dynamic_slice x20, local copies, waits for them, and re-layouts, delta_attention(): lax.scan(one_span, start_state, (recept, key_float, value_float, unit_key...  7.59 us
  transfers between devices with their start and end apart: 3, of which 1 were waited for; matrix products, arithmetic and copies ran while one was open for 56% of the time, Pallas kernels for 0%

commit v1 on v0

--- a/solution.py
+++ b/solution.py
@@ -41,7 +41,6 @@
     group_size = head_count // kv_count
     score_scale = HEAD ** (-0.5)
     own_first = lax.axis_index("sp") * row_count
-    forget_all = lax.all_gather(forget_rows, "sp", axis=0, tiled=True)
     forget_own = forget_rows.reshape(row_count, kv_count, group_size)
     query_heads = query_rows.reshape(row_count, kv_count, group_size, HEAD)
     query_pos = own_first + jnp.arange(row_count, dtype=jnp.int32)
@@ -50,7 +49,11 @@
         jnp.zeros((row_count, kv_count, group_size), jnp.float32),
         jnp.zeros((row_count, kv_count, group_size, HEAD), jnp.float32),
     )
-    key_piece = lax.all_gather(key_rows, "sp", axis=0, tiled=True)
+    forget_all, key_piece = jnp.split(
+        lax.all_gather(jnp.concatenate([forget_rows, key_rows], axis=1), "sp", axis=0, tiled=True),
+        [forget_rows.shape[1]],
+        axis=1,
+    )
     value_piece = lax.all_gather(value_rows, "sp", axis=0, tiled=True)
     piece_rows = key_piece.shape[0]
     block_rows = math.gcd(piece_rows, 512)

time: 231 us -> 224 us (0.970)
  blocking collectives: 71.9 us -> 59.8 us
  other arithmetic: 85.3 us -> 87.9 us
    all_gather x2 -> x1, blocking collectives: 27.7 us -> 15.5 us  [forget_attention(): lax.all_gather(jnp.concatenate([forget_rows, key_rows], axis=1), 'sp', ax...]
  transfers between devices with their start and end apart: 3 -> 3, of which waited for: 1 -> 1; matrix products, arithmetic and copies ran while one was open for 56% -> 60% of each run, Pallas kernels for 0% -> 0%
where the time goes in v1:
time: 224 us; the launch traced here: 223 us
  other arithmetic  87.9 us (39%)
  blocking collectives  59.8 us (27%)
  matrix products  30.9 us (14%)
  local copies, waits for them, and re-layouts  18.5 us (8%)
  between operations  13.5 us (6%)
  waiting for transfers between devices  11.6 us (5%)
    another operation x12, other arithmetic, one_span(): jax.scipy.linalg.solve_triangular(identity_span - mix_erase, right_side,...  79 us
    all_gather x2, blocking collectives, carried_in(): lax.all_gather(a.astype(kind), axis)  30.2 us
    dot_general x44, matrix products, product(): return jnp.einsum(form, left, right, precision=HIGHEST)  16.7 us
    all_gather x1, blocking collectives, forget_attention(): lax.all_gather(jnp.concatenate([forget_rows, key_rows], axis=1), 'sp', ax...  15.5 us
    all_gather x1, blocking collectives, forget_attention(): value_piece = lax.all_gather(value_rows, 'sp', axis=0, tiled=True)  14.1 us
    reduce_scatter x1, waiting for transfers between devices, shards(): lax.psum_scatter(round_half(partial_value).astype(jnp.bfloat16), 'tp', sc...  10.2 us
    dynamic_slice x20, local copies, waits for them, and re-layouts, delta_attention(): lax.scan(one_span, start_state, (recept, key_float, value_float, unit_key...  7.59 us
  transfers between devices with their start and end apart: 3, of which 1 were waited for; matrix products, arithmetic and copies ran while one was open for 60% of the time, Pallas kernels for 0%

profile of v1, /device:TPU:0, one launch (start us, length us, event | category | flops | bytes accessed | tf_op | source)
XLA Modules:
  0.0 223.0 jit_solution(17254553038363002301)
XLA Ops:
  6.5 0.7 all-gather.6.cloned.1.call-update
  7.3 0.7 all-gather.8.cloned.1.call-update
  8.1 1.2 reshape.167
  10.2 1.0 reshape.166
  11.3 1.0 neg.24
  13.0 106.6 %while.46 = (s32[]{:T(128)}, f32[4,128,64]{1,2,0:T(8,128)S(1)}, f32[4,4,64,128]{3,2,1,0:T(8,128)}, f32[4,4,64,64]{3,1,2,0:T(4,128)}, f32[4,4,64,64]{3,1,2,0:T(4,...) while((s32[]{:T(128)}, f32[4,128,64]{1,2,0:T(8,128)S(1)}, ...), condition=%wide.region_10.11_spmd.clone.clone, body=%wide.region_8.10_spmd.clone.clone.sunk | while | flops 253308992 | bytes 5993869 | solution.py:178
  13.0 0.9 constant_dynamic-slice_fusion.20
  14.1 0.9 constant_dynamic-slice_fusion.19
  15.6 19.7 %custom-call.11 = f32[4,1,64,64]{2,3,1,0:T(8,128)S(1)} custom-call(f32[4,1,64,64]{3,2,1,0:T(8,128)S(1)} %fusion.172), custom_call_target="InvertDiagBlocksLowerTriangular" | custom-call | tf_op jit(solution)/shard_map/while/body/eval_jaxpr/jit(_solve_triangular)/vmap()/triangular_solve | solution.py:161
  37.9 0.9 fusion.176
  39.6 0.9 constant_dynamic-slice_fusion.20
  40.7 0.9 constant_dynamic-slice_fusion.19
  42.2 19.7 %custom-call.11 = f32[4,1,64,64]{2,3,1,0:T(8,128)S(1)} custom-call(f32[4,1,64,64]{3,2,1,0:T(8,128)S(1)} %fusion.172), custom_call_target="InvertDiagBlocksLowerTriangular" | custom-call | tf_op jit(solution)/shard_map/while/body/eval_jaxpr/jit(_solve_triangular)/vmap()/triangular_solve | solution.py:161
  64.5 0.9 fusion.176
  66.3 0.9 constant_dynamic-slice_fusion.20
  67.4 0.9 constant_dynamic-slice_fusion.19
  68.9 19.7 %custom-call.11 = f32[4,1,64,64]{2,3,1,0:T(8,128)S(1)} custom-call(f32[4,1,64,64]{3,2,1,0:T(8,128)S(1)} %fusion.172), custom_call_target="InvertDiagBlocksLowerTriangular" | custom-call | tf_op jit(solution)/shard_map/while/body/eval_jaxpr/jit(_solve_triangular)/vmap()/triangular_solve | solution.py:161
  91.2 0.9 fusion.176
  92.9 0.9 constant_dynamic-slice_fusion.20
  94.0 0.9 constant_dynamic-slice_fusion.19
  95.5 19.7 %custom-call.11 = f32[4,1,64,64]{2,3,1,0:T(8,128)S(1)} custom-call(f32[4,1,64,64]{3,2,1,0:T(8,128)S(1)} %fusion.172), custom_call_target="InvertDiagBlocksLowerTriangular" | custom-call | tf_op jit(solution)/shard_map/while/body/eval_jaxpr/jit(_solve_triangular)/vmap()/triangular_solve | solution.py:161
  117.8 0.9 fusion.176
  119.7 15.7 %all-gather.1 = bf16[16,64,64]{2,1,0:T(8,128)(2,1)S(1)} all-gather(bf16[4,64,64]{2,1,0:T(8,128)(2,1)S(1)} %get-tuple-element.530), channel_id=3, replica_groups=mesh['sp'=4,'fs'=4,'tp'=2] {'sp'}, dimensions={0}, use_global_device_ids=true | all-gather | bytes 163840 | tf_op jit(solution)/shard_map/all_gather | solution.py:16
  135.4 14.6 %all-gather.2 = bf16[16,64,64]{2,1,0:T(8,128)(2,1)S(1)} all-gather(bf16[4,64,64]{2,1,0:T(8,128)(2,1)S(1)} %get-tuple-element.529), channel_id=4, replica_groups=mesh['sp'=4,'fs'=4,'tp'=2] {'sp'}, dimensions={0}, use_global_device_ids=true | all-gather | bytes 163840 | tf_op jit(solution)/shard_map/all_gather | solution.py:16
  150.0 1.0 copy-done
  151.3 1.7 fusion.65
  154.2 0.8 copy.72
  155.3 14.1 %all-gather = bf16[1,1024,128]{1,2,0:T(8,128)(2,1)S(1)} all-gather(bf16[1,256,128]{1,2,0:T(8,128)(2,1)S(1)} %copy.56), channel_id=2, replica_groups=mesh['sp'=4,'fs'=4,'tp'=2] {'sp'}, dimensions={1}, use_global_device_ids=true | all-gather | bytes 327680 | tf_op jit(solution)/shard_map/all_gather | solution.py:57
  169.4 15.5 %all_gather.24 = f32[1024,132]{0,1:T(8,128)S(1)} all-gather(f32[256,132]{0,1:T(8,128)S(1)} %pad_maximum_fusion), channel_id=1, replica_groups=mesh['sp'=4,'fs'=4,'tp'=2] {'sp'}, dimensions={0}, use_global_device_ids=true | all-gather | bytes 675840 | tf_op jit(solution)/shard_map/all_gather | solution.py:53
  184.9 15.0 %conditional.1 = (f32[256,2,2]{0,2,1:T(2,128)}, f32[256,2,2,64]{0,3,2,1:T(8,128)}) conditional(s32[]{:T(128)} %convert_element_type.64, () %tuple.38, (f32[1024,132]{0,1:T(8,128)S(1)}, s32[]{:T(128)}, s32[256]{0:T(256)S(1)}, bf16[1,256,256]{2,1,0:T(8,128)(2,1)S(1)}, f32[1,256,4]{1,2,0:T(4,128)S(1)}, /*index=5*/bf16[1024,128]{0,1:T(8,128)(2,1)S(1)}) %tuple.143), branch_computations={%region_0.0_spmd, %region_1.6_spmd} | conditional | flops 140318464 | bytes 9219459 | solution.py:104
  185.0 0.6 split.7
  186.2 0.7 copy.57
  187.5 12.4 %while.44 = (s32[]{:T(128)}, f32[256,2,2]{0,2,1:T(2,128)S(1)}, f32[256,2,2]{0,2,1:T(2,128)}, f32[256,2,2,64]{0,3,2,1:T(8,128)}, s32[256]{0:T(256)}, /*index=5*/b...) while((s32[]{:T(128)}, f32[256,2,2]{0,2,1:T(2,128)S(1)}, ...), condition=%wide.wide.region_5.5_spmd.clone, body=%wide.wide.region_2.4_spmd.clone.sunk | while | flops 140318208 | bytes 8373459 | solution.py:99
  187.6 0.7 constant_dynamic-slice_fusion.22
  188.3 0.8 broadcast_compare_fusion.3
  189.1 1.6 fusion.181
  191.1 0.6 fusion.184
  191.8 1.2 fusion.185
  193.0 0.7 constant_dynamic-slice_fusion.22
  193.7 0.8 broadcast_compare_fusion.3
  194.5 1.6 fusion.181
  196.5 1.3 fusion.184
  197.8 2.1 fusion.185
  200.0 1.0 multiply_reduce_fusion.2
  201.1 0.8 fusion.59
  201.9 1.7 fusion.67
  203.6 2.7 %fusion.54 = bf16[256,2048]{1,0:T(8,128)(2,1)} fusion(f32[256,2048]{1,0:T(8,128)S(1)} %fusion.67, bf16[256,2048]{1,0:T(8,128)(2,1)} %all-gather.8.cloned.1.call-done, f32[256,256]{1,0:T(8,128)S(1)} %copy.73, f32[256,256]{1,0:T(8,128)S(1)} %reshape.162, f32[256,256]{1,0:T(8,128)S(1)} %copy-done.1, f32[256]{0:T(256)S(1)} %copy-done.11), kind=kOutput, calls=%fused_computation.87 | convolution fusion | flops 269746176 | bytes 4981760 | tf_op jit(solution)/shard_map/dot_general | solution.py:230
  206.3 10.2 %reduce-scatter.2.cloned.1.call-done = bf16[128,2048]{1,0:T(8,128)(2,1)} async-done(((bf16[256,2048]{1,0:T(8,128)(2,1)}), bf16[128,2048]{1,0:T(8,128)(2,1)}) %reduce-scatter.2.cloned.1.call-update) | async-done | bytes 524304 | tf_op jit(solution)/shard_map/reduce_scatter | solution.py:231
  (166 shorter events, 21.9 us)
Async XLA Ops:
  6.5 3.6 %copy-start.3 = (bf16[1,256,256]{2,1,0:T(8,128)(2,1)S(1)}, bf16[1,256,256]{2,1,0:T(8,128)(2,1)}, u32[]{:S(2)}) copy-start(bf16[1,256,256]{2,1,0:T(8,128)(2,1)} %param.29) | copy-start | bytes 393220
  6.5 195.3 %all-gather.6.cloned.1.call-start = ((), (), s32[]{:S(2)}) async-start(), calls=%async_computation.1 | async-start | bytes 1310720 | tf_op jit(solution)/shard_map/all_gather | solution.py:226
  7.3 4.0 %copy-start.2 = (f32[1,256,256]{2,1,0:T(8,128)S(1)}, f32[1,256,256]{2,1,0:T(8,128)}, u32[]{:S(2)}) copy-start(f32[1,256,256]{2,1,0:T(8,128)} %param.30) | copy-start | bytes 786436
  7.3 196.3 %all-gather.8.cloned.1.call-start = ((), (), s32[]{:S(2)}) async-start(), calls=%async_computation.2 | async-start | bytes 1310720 | tf_op jit(solution)/shard_map/all_gather | solution.py:227
  8.0 208.5 %reduce-scatter.2.cloned.1.call-start = ((), (), s32[]{:S(2)}) async-start(), calls=%async_computation.3 | async-start | bytes 1572864 | tf_op jit(solution)/shard_map/reduce_scatter | solution.py:231
  9.6 2.7 %copy-start.4 = (bf16[1,256,256]{2,1,0:T(8,128)(2,1)S(1)}, bf16[1,256,256]{2,1,0:T(8,128)(2,1)}, u32[]{:S(2)}) copy-start(bf16[1,256,256]{2,1,0:T(8,128)(2,1)} %param.28) | copy-start | bytes 393220
  9.7 2.9 %copy-start.5 = (bf16[1,256,256]{2,1,0:T(8,128)(2,1)S(1)}, bf16[1,256,256]{2,1,0:T(8,128)(2,1)}, u32[]{:S(2)}) copy-start(bf16[1,256,256]{2,1,0:T(8,128)(2,1)} %param.26) | copy-start | bytes 393220
  149.9 1.0 copy-start
  153.1 1.9 copy-start.7
  153.1 2.0 copy-start.8
  153.4 16.0 %copy-start.9 = (f32[1,256,4]{1,2,0:T(4,128)S(1)}, f32[1,256,4]{1,2,0:T(4,128)}, u32[]{:S(2)}) copy-start(f32[1,256,4]{1,2,0:T(4,128)} %param.24) | copy-start | bytes 12292
  153.5 31.5 %copy-start.6 = (bf16[1,256,256]{2,1,0:T(8,128)(2,1)S(1)}, bf16[1,256,256]{2,1,0:T(8,128)(2,1)}, u32[]{:S(2)}) copy-start(bf16[1,256,256]{2,1,0:T(8,128)(2,1)} %param.21) | copy-start | bytes 393220
  184.9 2.6 %copy-start.10 = (f32[1,256,4]{1,2,0:T(4,128)}, f32[1,256,4]{1,2,0:T(4,128)S(1)}, u32[]{:S(2)}) copy-start(f32[1,256,4]{1,2,0:T(4,128)S(1)} %get-tuple-element.786) | copy-start | bytes 12292 | tf_op jit(solution)/shard_map/cond
  200.0 3.6 %copy-start.1 = (f32[256,256]{1,0:T(8,128)S(1)}, f32[256,256]{1,0:T(8,128)}, u32[]{:S(2)}) copy-start(f32[256,256]{1,0:T(8,128)} %copy.72) | copy-start | bytes 786436
  200.0 3.6 %copy-start.11 = (f32[256]{0:T(256)S(1)}, f32[256]{0:T(256)}, u32[]{:S(2)}) copy-start(f32[256]{0:T(256)} %param.31) | copy-start | bytes 3076
Sparse Core Ops, SparseCore 0:
  9.2 29.8 all-gather.5
  40.9 27.0 all-gather.7
  206.4 10.0 reduce-scatter.1
